TPU v7x, 32 devices: a whole 2x2x4 slice. The times are simulated.
32 devices in a mesh: sp: 8 (over z, x), tp: 4 (over y, core).
Axes of the slice: x: 2, y: 2, z: 4, core: 2. Of those that a mesh axis runs over, the one named last changes fastest.
Arguments:
- lane_source_signal: bfloat16 [1024, 1024], P('tp', 'sp'), may hold values from -6 to 6
- spectral_damping_part: float32 [64, 64], P('tp'), may hold values from -3 to -0.0002
- spectral_angular_part: float32 [64, 64], P('tp'), may hold values from 0.31 to 201.0624
- interval_exponent: float32 [64], P('tp'), may hold values from -3.9 to -1.6
- entry_matrix_inphase: float32 [64, 64, 16], P('tp'), may hold values from -1 to 1
- entry_matrix_quadrature: float32 [64, 64, 16], P('tp'), may hold values from -1 to 1
- emission_inphase: float32 [64, 16, 64], P('tp'), may hold values from -0.75 to 0.75
- emission_quadrature: float32 [64, 16, 64], P('tp'), may hold values from -0.75 to 0.75
- lane_bypass_factor: float32 [1024], P('tp'), may hold values from -5 to 5
- spike_shrink_offset: float32 [64, 1024], P('tp', 'sp'), may hold values from -1.4 to 0
- lane_exit_matrix: bfloat16 [1024, 4096], P('tp'), may hold values from -0.1875 to 0.1875
- skipline_stream: bfloat16 [1024, 4096], P('sp'), may hold values from -6 to 6
- specialist_scaling_vector: float32 [4096], replicated, may hold values from 0.1 to 1.9
- selected_specialists: int32 [1024, 2], P('sp'), may hold values from 0 to 7, all different within a row; in each aligned block of 128 rows (0 to 127, 128 to 255, ...) at most 64 rows name the same one
- dispatcher_scores: float32 [1024, 2], P('sp'), may hold values from 0.1 to 1
- specialist_valve_matrix: bfloat16 [8, 4096, 2048], P('sp', None, 'tp'), may hold values from -0.09375 to 0.09375
- specialist_widen_matrix: bfloat16 [8, 4096, 2048], P('sp', None, 'tp'), may hold values from -0.09375 to 0.09375
- specialist_shrink_matrix: bfloat16 [8, 2048, 4096], P('sp', 'tp'), may hold values from -0.1875 to 0.1875
Outputs:
- updated: bfloat16 [1024, 4096], P('sp', 'tp')
Inputs may be any that keep to these rules, and one draw needn't show every extreme that they name: `selected_specialists`: each row names 2 different experts. Among the rows of each aligned block of 128 positions no expert is named more than 64 times, and in every block some expert is named exactly 64 times.
All inputs are finite; a program needn't handle non-finite values.
Results may differ from a plain program's by a relative error of at most 0.019.
Values may be sent and summed in bfloat16 or wider, within the bound.
No kernel may reach another device: no remote copies, remote signals or barrier semaphores. Data moves between devices by JAX's collectives and lax.ppermute only.
A program may use at most 64 MiB of HBM per device.

v0:
```python
import jax
import jax.numpy as jnp
from jax import lax
from jax.sharding import PartitionSpec as P

EPS = 1e-06
PRECISE_MODE = lax.Precision.HIGHEST


def carried_in(value, axis, join, neutral):
    count, mine = (lax.axis_size(axis), lax.axis_index(axis))
    pieces = jax.tree.map(lambda part: lax.all_gather(part, axis), value)
    running = jax.tree.map(
        lambda part, zero: jnp.full_like(part, 0) + jnp.asarray(zero, part.dtype), value, neutral
    )

    def lap(position, running):
        longer = join(running, jax.tree.map(lambda part: part[position], pieces))
        return jax.tree.map(lambda new, old: jnp.where(position < mine, new, old), longer, running)

    return lax.fori_loop(0, count - 1, lap, running)


def affine_pair(earlier, latter):
    mul_re = earlier[0] * latter[0] - earlier[1] * latter[1]
    mul_im = earlier[0] * latter[1] + earlier[1] * latter[0]
    add_re = latter[0] * earlier[2] - latter[1] * earlier[3] + latter[2]
    add_im = latter[0] * earlier[3] + latter[1] * earlier[2] + latter[3]
    return (mul_re, mul_im, add_re, add_im)


def local_prefix(elements):
    length = elements[0].shape[2]
    fills = (1.0, 0.0, 0.0, 0.0)
    offset = 1
    while offset < length:
        earlier = tuple(
            (
                jnp.pad(
                    item[:, :, : length - offset],
                    ((0, 0), (0, 0), (offset, 0)),
                    constant_values=fill,
                )
                for item, fill in zip(elements, fills)
            )
        )
        elements = affine_pair(earlier, elements)
        offset = offset * 2
    return elements


def full_norm(projected, skipline_stream, specialist_scaling_vector, col_start, d_local):
    stream = (
        skipline_stream.astype(jnp.float32)
        + lax.optimization_barrier(projected).astype(jnp.float32)
    ).astype(jnp.bfloat16)
    stream_f = lax.optimization_barrier(stream).astype(jnp.float32)
    inv_rms = lax.rsqrt(jnp.mean(stream_f * stream_f, axis=-1, keepdims=True) + EPS)
    normed = (stream_f * inv_rms * specialist_scaling_vector).astype(jnp.bfloat16)
    own_stream = lax.dynamic_slice_in_dim(stream_f, col_start, d_local, 1)
    own_cols = lax.dynamic_slice_in_dim(normed, col_start, d_local, 1)
    return (own_stream, normed, own_cols)


def per_device(
    lane_source_signal,
    spectral_damping_part,
    spectral_angular_part,
    interval_exponent,
    entry_matrix_inphase,
    entry_matrix_quadrature,
    emission_inphase,
    emission_quadrature,
    lane_bypass_factor,
    spike_shrink_offset,
    lane_exit_matrix,
    skipline_stream,
    specialist_scaling_vector,
    selected_specialists,
    dispatcher_scores,
    specialist_valve_matrix,
    specialist_widen_matrix,
    specialist_shrink_matrix,
):
    f32 = jnp.float32
    bf16 = jnp.bfloat16
    groups_here = spectral_damping_part.shape[0]
    lanes_within_bundle = entry_matrix_inphase.shape[2]
    tok_local = lane_source_signal.shape[1]
    bundled_signal = lane_source_signal.astype(f32).reshape(
        groups_here, lanes_within_bundle, tok_local
    )
    step_size = jnp.exp(interval_exponent)[:, None]
    natural_pace_exponent = spectral_damping_part * step_size
    angle = spectral_angular_part * step_size
    num_re = jnp.expm1(natural_pace_exponent) * jnp.cos(angle) - 2.0 * jnp.sin(0.5 * angle) ** 2
    num_im = jnp.exp(natural_pace_exponent) * jnp.sin(angle)
    denom = (
        spectral_damping_part * spectral_damping_part
        + spectral_angular_part * spectral_angular_part
    )
    fac_re = (num_re * spectral_damping_part + num_im * spectral_angular_part) / denom
    fac_im = (num_im * spectral_damping_part - num_re * spectral_angular_part) / denom
    map_re = (
        fac_re[:, :, None] * entry_matrix_inphase - fac_im[:, :, None] * entry_matrix_quadrature
    )
    map_im = (
        fac_re[:, :, None] * entry_matrix_quadrature + fac_im[:, :, None] * entry_matrix_inphase
    )
    drive_re = jnp.einsum("gpc,gct->gpt", map_re, bundled_signal, precision=PRECISE_MODE)
    drive_im = jnp.einsum("gpc,gct->gpt", map_im, bundled_signal, precision=PRECISE_MODE)
    recurrence_modulus = jnp.exp(
        natural_pace_exponent[:, :, None] + spike_shrink_offset[:, None, :]
    )
    trans_re = recurrence_modulus * jnp.cos(angle)[:, :, None]
    trans_im = recurrence_modulus * jnp.sin(angle)[:, :, None]
    cum_re, cum_im, state_real, state_imaginary = local_prefix(
        (trans_re, trans_im, drive_re, drive_im)
    )
    summary = (cum_re[:, :, -1], cum_im[:, :, -1], state_real[:, :, -1], state_imaginary[:, :, -1])
    unit = jnp.ones_like(summary[0])
    blank = jnp.zeros_like(summary[0])
    carried = carried_in(summary, "sp", affine_pair, (unit, blank, blank, blank))
    enter_re = carried[2][:, :, None]
    enter_im = carried[3][:, :, None]
    state_real = state_real + cum_re * enter_re - cum_im * enter_im
    state_imaginary = state_imaginary + cum_re * enter_im + cum_im * enter_re
    value = (
        jnp.einsum("nef,nfi->nei", emission_inphase, state_real, precision=PRECISE_MODE)
        - jnp.einsum("nef,nfi->nei", emission_quadrature, state_imaginary, precision=PRECISE_MODE)
        + lane_bypass_factor.reshape(groups_here, lanes_within_bundle)[:, :, None] * bundled_signal
    )
    recurrence_result = (
        jax.nn.gelu(value).astype(bf16).reshape(groups_here * lanes_within_bundle, tok_local)
    )
    width = specialist_scaling_vector.shape[0]
    d_local = width // lax.axis_size("tp")
    col_start = lax.axis_index("tp") * d_local
    partial_rows = jnp.einsum(
        "ct,cd->td", recurrence_result, lane_exit_matrix, preferred_element_type=f32
    )
    projected = lax.psum(partial_rows.astype(jnp.bfloat16), "tp").astype(jnp.float32).astype(bf16)
    own_stream, normed, own_cols = full_norm(
        projected, skipline_stream, specialist_scaling_vector, col_start, d_local
    )
    share = dispatcher_scores / jnp.sum(dispatcher_scores, axis=1, keepdims=True)
    experts = lax.axis_size("sp")
    top = selected_specialists.shape[1]
    capacity = 2 * tok_local * top // experts
    flat_routes = selected_specialists.reshape(-1)
    hits = (flat_routes[:, None] == jnp.arange(experts, dtype=jnp.int32)[None, :]).astype(jnp.int32)
    ranks = jnp.sum((jnp.cumsum(hits, axis=0) - hits) * hits, axis=1)
    slot_ids = flat_routes * capacity + ranks
    slot_grid = jnp.arange(experts * capacity, dtype=jnp.int32)
    matched = slot_grid[:, None] == slot_ids[None, :]
    token_of = jnp.arange(tok_local * top, dtype=jnp.int32) // top
    slot_token = jnp.sum(jnp.where(matched, token_of[None, :], 0), axis=1)
    slot_live = jnp.any(matched, axis=1)
    gate_w = specialist_valve_matrix[0]
    up_w = specialist_widen_matrix[0]
    down_w = specialist_shrink_matrix[0]
    bf_zero = jnp.zeros((), bf16)
    dispatch = jnp.where(slot_live[:, None], own_cols[slot_token], bf_zero).reshape(
        experts, capacity, d_local
    )
    arrived = lax.all_to_all(dispatch, "sp", split_axis=0, concat_axis=0, tiled=True)
    piece = lax.all_gather(arrived, "tp", axis=2, tiled=True)
    gate_part = jnp.einsum("snd,df->snf", piece, gate_w, preferred_element_type=f32)
    up_part = jnp.einsum("snd,df->snf", piece, up_w, preferred_element_type=f32)
    hidden = (jax.nn.silu(gate_part) * up_part).astype(bf16)
    flat_hidden = hidden.reshape(experts * capacity, hidden.shape[2])
    down_part = jnp.dot(flat_hidden, down_w, preferred_element_type=f32).astype(bf16)
    summed = lax.psum_scatter(
        down_part.astype(f32).astype(jnp.bfloat16), "tp", scatter_dimension=1, tiled=True
    ).astype(jnp.float32)
    expert_out = summed.astype(bf16).reshape(experts, capacity, d_local)
    returned = lax.all_to_all(expert_out, "sp", split_axis=0, concat_axis=0, tiled=True).reshape(
        experts * capacity, d_local
    )
    picked = returned[slot_ids].reshape(tok_local, top, d_local)
    combined = jnp.sum(lax.optimization_barrier(picked).astype(f32) * share[:, :, None], axis=1)
    return (own_stream + combined).astype(bf16)


def solution(mesh):
    placed = (
        P("tp", "sp"),
        P("tp", None),
        P("tp", None),
        P("tp"),
        P("tp", None, None),
        P("tp", None, None),
        P("tp", None, None),
        P("tp", None, None),
        P("tp"),
        P("tp", "sp"),
        P("tp", None),
        P("sp", None),
        P(),
        P("sp", None),
        P("sp", None),
        P("sp", None, "tp"),
        P("sp", None, "tp"),
        P("sp", "tp", None),
    )
    return jax.shard_map(
        per_device, mesh=mesh, in_specs=placed, out_specs=P("sp", "tp"), check_vma=False
    )
```

profile of v0, /device:TPU:0, one launch (start us, length us, event | category | flops | bytes accessed | tf_op | source)
XLA Modules:
  0.0 370.3 jit_solution(14271177628407040252)
XLA Ops:
  6.5 0.8 exp.13
  7.4 0.9 fusion.59
  8.2 1.6 fusion.45
  9.8 1.6 fusion.49
  11.4 1.4 subtract_add_fusion.6
  12.9 1.0 add_add_fusion.5
  13.9 0.3 subtract_add_fusion.5
  14.3 0.6 add_add_fusion.4
  14.9 0.3 subtract_add_fusion.4
  15.2 0.6 add_add_fusion.3
  15.8 0.3 subtract_add_fusion.3
  16.2 0.6 add_add_fusion.2
  16.8 0.3 subtract_add_fusion.2
  17.2 0.6 add_add_fusion.1
  18.1 1.4 add_add_fusion
  19.5 1.4 multiply_subtract_fusion
  20.9 1.0 slice.168
  21.9 1.3 copy.32
  23.2 32.4 %all-gather = f32[128,64,1]{1,2,0:T(1,128)S(1)} all-gather(f32[16,64,1]{1,2,0:T(1,128)S(1)} %copy.32), channel_id=2, replica_groups=mesh['sp'=8,'tp'=4] {'sp'}, dimensions={0}, use_global_device_ids=true | all-gather | bytes 36864 | tf_op jit(solution)/shard_map/all_gather | solution.py:12
  55.5 1.0 slice.169
  56.5 1.2 copy.33
  57.8 30.5 %all-gather.1 = f32[128,64,1]{1,2,0:T(1,128)S(1)} all-gather(f32[16,64,1]{1,2,0:T(1,128)S(1)} %copy.33), channel_id=3, replica_groups=mesh['sp'=8,'tp'=4] {'sp'}, dimensions={0}, use_global_device_ids=true | all-gather | bytes 36864 | tf_op jit(solution)/shard_map/all_gather | solution.py:12
  88.3 2.0 slice.170
  90.4 1.2 copy.34
  91.6 30.5 %all-gather.2 = f32[128,64,1]{1,2,0:T(1,128)S(1)} all-gather(f32[16,64,1]{1,2,0:T(1,128)S(1)} %copy.34), channel_id=4, replica_groups=mesh['sp'=8,'tp'=4] {'sp'}, dimensions={0}, use_global_device_ids=true | all-gather | bytes 36864 | tf_op jit(solution)/shard_map/all_gather | solution.py:12
  122.2 2.0 slice.171
  124.2 1.2 copy.35
  125.4 30.5 %all-gather.3 = f32[128,64,1]{1,2,0:T(1,128)S(1)} all-gather(f32[16,64,1]{1,2,0:T(1,128)S(1)} %copy.35), channel_id=5, replica_groups=mesh['sp'=8,'tp'=4] {'sp'}, dimensions={0}, use_global_device_ids=true | all-gather | bytes 36864 | tf_op jit(solution)/shard_map/all_gather | solution.py:12
  156.4 1.9 fusion.22
  158.2 1.9 fusion.42
  160.1 1.5 convolution_convert_fusion.1
  162.3 0.6 reduce-window.6
  163.7 35.4 %all-reduce.30.cloned.1.call-done = bf16[128,4096]{1,0:T(8,128)(2,1)} async-done(((bf16[128,4096]{1,0:T(8,128)(2,1)}), bf16[128,4096]{1,0:T(8,128)(2,1)}) %all-reduce.30.cloned.1.call-update) | async-done | bytes 1048592 | tf_op jit(solution)/shard_map/psum | solution.py:142
  199.0 1.8 add_convert_fusion
  201.3 1.0 copy-done.1
  202.5 2.1 gather_fusion
  204.7 30.6 %all_to_all.10 = bf16[8,64,1024]{2,1,0:T(8,128)(2,1)} all-to-all(bf16[8,64,1024]{2,1,0:T(8,128)(2,1)S(1)} %broadcast_select_fusion), channel_id=1, replica_groups=mesh['sp'=8,'tp'=4] {'sp'}, dimensions={0} | all-to-all | bytes 2097152 | tf_op jit(solution)/shard_map/all_to_all | solution.py:166
  235.4 33.4 %all-gather.6.cloned.1.call-done = bf16[8,64,4096]{2,1,0:T(8,128)(2,1)} async-done(((bf16[8,64,1024]{2,1,0:T(8,128)(2,1)}), bf16[8,64,4096]{2,1,0:T(8,128)(2,1)}) %all-gather.6.cloned.1.call-update) | async-done | bytes 4194320 | tf_op jit(solution)/shard_map/all_gather | solution.py:167
  268.9 5.9 %fusion.7 = f32[8,64,512]{2,1,0:T(8,128)S(1)} fusion(bf16[8,64,4096]{2,1,0:T(8,128)(2,1)} %all-gather.6.cloned.1.call-done, bf16[1,4096,512]{2,1,0:T(8,128)(2,1)} %param.35), kind=kOutput, calls=%fused_computation.17 | convolution fusion | flops 2147483648 | bytes 9437184 | tf_op jit(solution)/shard_map/snd,df->snf/dot_general | solution.py:168
  274.8 2.4 fusion.12
  277.3 4.3 %convolution_convert_fusion = bf16[512,4096]{1,0:T(8,128)(2,1)} fusion(bf16[512,512]{1,0:T(8,128)(2,1)S(1)} %bitcast.169, bf16[1,512,4096]{2,1,0:T(8,128)(2,1)S(1)} %copy-done.8), kind=kOutput, calls=%fused_computation.12 | convolution fusion | flops 2149580800 | bytes 8912896 | tf_op jit(solution)/shard_map/dot_general | solution.py:172
  281.6 44.6 %reduce-scatter.2.cloned.1.call-done = bf16[512,1024]{1,0:T(8,128)(2,1)} async-done(((bf16[512,4096]{1,0:T(8,128)(2,1)}), bf16[512,1024]{1,0:T(8,128)(2,1)}) %reduce-scatter.2.cloned.1.call-update) | async-done | bytes 1048592 | tf_op jit(solution)/shard_map/reduce_scatter | solution.py:173
  326.1 5.5 %all-to-all-start.1 = ((bf16[8,64,1024]{2,1,0:T(8,128)(2,1)}), bf16[8,64,1024]{2,1,0:T(8,128)(2,1)S(1)}, u32[]{:S(2)}, u32[]{:S(2)}) async-start(bf16[8,64,1024]{2,1,0:T(8,128)(2,1)} %bitcast.156), calls=%async_computation.2 | async-start | bytes 2097152 | tf_op jit(solution)/shard_map/all_to_all | solution.py:177
  332.1 25.2 %all-to-all-done.1 = bf16[8,64,1024]{2,1,0:T(8,128)(2,1)S(1)} async-done(((bf16[8,64,1024]{2,1,0:T(8,128)(2,1)}), bf16[8,64,1024]{2,1,0:T(8,128)(2,1)S(1)}, u32[]{:S(2)}, u32[]{:S(2)}) %all-to-all-start.1) | async-done | bytes 1048608 | tf_op jit(solution)/shard_map/all_to_all | solution.py:177
  357.3 2.0 gather_fusion.1
  359.3 1.2 reshape.140
  360.5 1.4 multiply_reduce_fusion.1
  361.9 1.8 add_convert_fusion.1
  (66 shorter events, 3.4 us)
Async XLA Ops:
  6.5 153.6 %copy-start = (bf16[256,4096]{1,0:T(8,128)(2,1)S(1)}, bf16[256,4096]{1,0:T(8,128)(2,1)}, u32[]{:S(2)}) copy-start(bf16[256,4096]{1,0:T(8,128)(2,1)} %param.30) | copy-start | bytes 6291460
  6.5 6.3 %copy-start.3 = (f32[16,128]{1,0:T(8,128)S(1)}, f32[16,128]{1,0:T(8,128)}, u32[]{:S(2)}) copy-start(f32[16,128]{1,0:T(8,128)} %param.29) | copy-start | bytes 24580
  6.5 192.5 %all-reduce.30.cloned.1.call-start = ((), (), s32[]{:S(2)}) async-start(), calls=%async_computation.3 | async-start | bytes 2097152 | tf_op jit(solution)/shard_map/psum | solution.py:142
  20.9 135.3 %copy-start.6 = (f32[256]{0:T(256)S(1)}, f32[256]{0:T(256)}, u32[]{:S(2)}) copy-start(f32[256]{0:T(256)} %param.28) | copy-start | bytes 3076
  21.9 136.3 %copy-start.2 = (bf16[256,128]{1,0:T(8,128)(2,1)S(1)}, bf16[256,128]{1,0:T(8,128)(2,1)}, u32[]{:S(2)}) copy-start(bf16[256,128]{1,0:T(8,128)(2,1)} %param.20) | copy-start | bytes 196612
  156.3 5.6 %copy-start.4 = (s32[128,2]{0,1:T(2,128)S(1)}, s32[128,2]{0,1:T(2,128)}, u32[]{:S(2)}) copy-start(s32[128,2]{0,1:T(2,128)} %param.33) | copy-start | bytes 3076
  161.6 107.2 %all-gather.6.cloned.1.call-start = ((), (), s32[]{:S(2)}) async-start(), calls=%async_computation.4 | async-start | bytes 5242880 | tf_op jit(solution)/shard_map/all_gather | solution.py:167
  163.5 38.9 %dynamic-slice-start = ((f32[4096]{0:T(1024)}, s32[]{:T(128)}), f32[1024]{0:T(1024)S(1)}, s32[]{:S(2)}) async-start(f32[4096]{0:T(1024)} %param.32, s32[]{:T(128)} %select_n.74), calls=%async_computation.6 | async-start | bytes 8704 | tf_op jit(solution)/shard_map/dynamic_slice | solution.py:61
  201.0 1.3 copy-start.1
  235.4 90.8 %reduce-scatter.2.cloned.1.call-start = ((), (), s32[]{:S(2)}) async-start(), calls=%async_computation.5 | async-start | bytes 5242880 | tf_op jit(solution)/shard_map/reduce_scatter | solution.py:173
  268.8 5.9 %copy-start.7 = (bf16[1,4096,512]{2,1,0:T(8,128)(2,1)S(1)}, bf16[1,4096,512]{2,1,0:T(8,128)(2,1)}, u32[]{:S(2)}) copy-start(bf16[1,4096,512]{2,1,0:T(8,128)(2,1)} %param.36) | copy-start | bytes 12582916
  268.9 5.9 %copy-start.9 = (bf16[8,64,4096]{2,1,0:T(8,128)(2,1)S(1)}, bf16[8,64,4096]{2,1,0:T(8,128)(2,1)}, u32[]{:S(2)}) copy-start(bf16[8,64,4096]{2,1,0:T(8,128)(2,1)} %all-gather.6.cloned.1.call-done) | copy-start | bytes 12582916
  274.8 2.5 copy-start.8
  281.6 50.4 %copy-start.5 = (f32[128,2]{0,1:T(2,128)S(1)}, f32[128,2]{0,1:T(2,128)}, u32[]{:S(2)}) copy-start(f32[128,2]{0,1:T(2,128)} %param.34) | copy-start | bytes 3076
  326.1 31.2 %all-to-all-start.1 = ((bf16[8,64,1024]{2,1,0:T(8,128)(2,1)}), bf16[8,64,1024]{2,1,0:T(8,128)(2,1)S(1)}, u32[]{:S(2)}, u32[]{:S(2)}) async-start(bf16[8,64,1024]{2,1,0:T(8,128)(2,1)} %bitcast.156), calls=%async_computation.2 | async-start | bytes 2097152 | tf_op jit(solution)/shard_map/all_to_all | solution.py:177
Sparse Core Ops, SparseCore 0:
  161.8 37.2 all-reduce.29
  235.5 33.3 all-gather.5
  281.7 44.3 reduce-scatter.1
where the time goes:
time: 371 us; the launch traced here: 370 us
  blocking collectives  155 us (42%)
  waiting for transfers between devices  139 us (37%)
  matrix products  21 us (6%)
  local copies, waits for them, and re-layouts  19.4 us (5%)
  other arithmetic  17.3 us (5%)
  between operations  13.5 us (4%)
  starting transfers between devices  5.77 us (2%)
    all_gather x4, blocking collectives, carried_in(): pieces = jax.tree.map(lambda part: lax.all_gather(part, axis), value)  124 us
    reduce_scatter x1, waiting for transfers between devices, per_device(): lax.psum_scatter(down_part.astype(f32).astype(jnp.bfloat16), 'tp', scatte...  44.6 us
    psum x1, waiting for transfers between devices, per_device(): lax.psum(partial_rows.astype(jnp.bfloat16), 'tp').astype(jnp.float32)  35.4 us
    all_gather x1, waiting for transfers between devices, per_device(): piece = lax.all_gather(arrived, 'tp', axis=2, tiled=True)  33.4 us
    all_to_all x1, blocking collectives, per_device(): lax.all_to_all(dispatch, 'sp', split_axis=0, concat_axis=0, tiled=True)  30.6 us
    all_to_all x1, waiting for transfers between devices, per_device(): lax.all_to_all(expert_out, 'sp', split_axis=0, concat_axis=0, tiled=True)  25.2 us
  transfers between devices with their start and end apart: 4, of which 4 were waited for; matrix products, arithmetic and copies ran while one was open for 1% of the time, Pallas kernels for 0%

commit v1 on v0

--- a/solution.py
+++ b/solution.py
@@ -164,7 +164,7 @@
         experts, capacity, d_local
     )
     arrived = lax.all_to_all(dispatch, "sp", split_axis=0, concat_axis=0, tiled=True)
-    piece = lax.all_gather(arrived, "tp", axis=2, tiled=True)
+    piece = jnp.concatenate(lax.all_gather(arrived, "tp"), axis=2)
     gate_part = jnp.einsum("snd,df->snf", piece, gate_w, preferred_element_type=f32)
     up_part = jnp.einsum("snd,df->snf", piece, up_w, preferred_element_type=f32)
     hidden = (jax.nn.silu(gate_part) * up_part).astype(bf16)

time: 371 us -> 371 us (level)
  no operation moved by 1% of the time
where the time goes in v1:
time: 371 us; the launch traced here: 370 us
  blocking collectives  155 us (42%)
  waiting for transfers between devices  139 us (37%)
  local copies, waits for them, and re-layouts  22.8 us (6%)
  matrix products  17.4 us (5%)
  other arithmetic  17.3 us (5%)
  between operations  13.5 us (4%)
  starting transfers between devices  5.78 us (2%)
    all_gather x4, blocking collectives, carried_in(): pieces = jax.tree.map(lambda part: lax.all_gather(part, axis), value)  124 us
    reduce_scatter x1, waiting for transfers between devices, per_device(): lax.psum_scatter(down_part.astype(f32).astype(jnp.bfloat16), 'tp', scatte...  44.6 us
    psum x1, waiting for transfers between devices, per_device(): lax.psum(partial_rows.astype(jnp.bfloat16), 'tp').astype(jnp.float32)  35.4 us
    all_gather x1, waiting for transfers between devices, per_device(): piece = jnp.concatenate(lax.all_gather(arrived, 'tp'), axis=2)  33.4 us
    all_to_all x1, blocking collectives, per_device(): lax.all_to_all(dispatch, 'sp', split_axis=0, concat_axis=0, tiled=True)  30.6 us
    all_to_all x1, waiting for transfers between devices, per_device(): lax.all_to_all(expert_out, 'sp', split_axis=0, concat_axis=0, tiled=True)  25.2 us
  transfers between devices with their start and end apart: 4, of which 4 were waited for; matrix products, arithmetic and copies ran while one was open for 1% of the time, Pallas kernels for 0%

profile of v1, /device:TPU:0, one launch (start us, length us, event | category | flops | bytes accessed | tf_op | source)
XLA Modules:
  0.0 370.1 jit_solution(10829734964338050824)
XLA Ops:
  6.5 0.8 exp.13
  7.4 0.9 fusion.59
  8.2 1.6 fusion.45
  9.8 1.6 fusion.49
  11.4 1.4 subtract_add_fusion.6
  12.9 1.0 add_add_fusion.5
  13.9 0.3 subtract_add_fusion.5
  14.3 0.6 add_add_fusion.4
  14.9 0.3 subtract_add_fusion.4
  15.2 0.6 add_add_fusion.3
  16.2 0.6 add_add_fusion.2
  17.2 0.6 add_add_fusion.1
  18.1 1.4 add_add_fusion
  19.5 1.4 multiply_subtract_fusion
  20.9 1.0 slice.168
  21.9 1.3 copy.34
  23.2 32.4 %all-gather = f32[128,64,1]{1,2,0:T(1,128)S(1)} all-gather(f32[16,64,1]{1,2,0:T(1,128)S(1)} %copy.34), channel_id=2, replica_groups=mesh['sp'=8,'tp'=4] {'sp'}, dimensions={0}, use_global_device_ids=true | all-gather | bytes 36864 | tf_op jit(solution)/shard_map/all_gather | solution.py:12
  55.5 1.0 slice.169
  56.5 1.2 copy.35
  57.8 30.5 %all-gather.1 = f32[128,64,1]{1,2,0:T(1,128)S(1)} all-gather(f32[16,64,1]{1,2,0:T(1,128)S(1)} %copy.35), channel_id=3, replica_groups=mesh['sp'=8,'tp'=4] {'sp'}, dimensions={0}, use_global_device_ids=true | all-gather | bytes 36864 | tf_op jit(solution)/shard_map/all_gather | solution.py:12
  88.3 2.0 slice.170
  90.4 1.2 copy.36
  91.6 30.5 %all-gather.2 = f32[128,64,1]{1,2,0:T(1,128)S(1)} all-gather(f32[16,64,1]{1,2,0:T(1,128)S(1)} %copy.36), channel_id=4, replica_groups=mesh['sp'=8,'tp'=4] {'sp'}, dimensions={0}, use_global_device_ids=true | all-gather | bytes 36864 | tf_op jit(solution)/shard_map/all_gather | solution.py:12
  122.2 2.0 slice.171
  124.2 1.2 copy.37
  125.4 30.5 %all-gather.3 = f32[128,64,1]{1,2,0:T(1,128)S(1)} all-gather(f32[16,64,1]{1,2,0:T(1,128)S(1)} %copy.37), channel_id=5, replica_groups=mesh['sp'=8,'tp'=4] {'sp'}, dimensions={0}, use_global_device_ids=true | all-gather | bytes 36864 | tf_op jit(solution)/shard_map/all_gather | solution.py:12
  156.4 1.9 fusion.22
  158.2 1.9 fusion.42
  160.1 1.5 convolution_convert_fusion.1
  162.3 0.6 reduce-window.6
  163.7 35.4 %all-reduce.30.cloned.1.call-done = bf16[128,4096]{1,0:T(8,128)(2,1)} async-done(((bf16[128,4096]{1,0:T(8,128)(2,1)}), bf16[128,4096]{1,0:T(8,128)(2,1)}) %all-reduce.30.cloned.1.call-update) | async-done | bytes 1048592 | tf_op jit(solution)/shard_map/psum | solution.py:142
  199.0 1.8 add_convert_fusion
  201.3 1.0 copy-done.1
  202.5 2.1 gather_fusion
  204.7 30.6 %all_to_all.10 = bf16[8,64,1024]{2,1,0:T(8,128)(2,1)} all-to-all(bf16[8,64,1024]{2,1,0:T(8,128)(2,1)S(1)} %broadcast_select_fusion), channel_id=1, replica_groups=mesh['sp'=8,'tp'=4] {'sp'}, dimensions={0} | all-to-all | bytes 2097152 | tf_op jit(solution)/shard_map/all_to_all | solution.py:166
  235.4 33.4 %all-gather.7.cloned.1.call-done = bf16[32,64,1024]{2,1,0:T(8,128)(2,1)} async-done(((bf16[8,64,1024]{2,1,0:T(8,128)(2,1)}), bf16[32,64,1024]{2,1,0:T(8,128)(2,1)}) %all-gather.7.cloned.1.call-update) | async-done | bytes 4194320 | tf_op jit(solution)/shard_map/all_gather | solution.py:167
  268.9 2.8 copy.43
  271.7 0.6 copy-done.7
  272.3 2.3 fusion.7
  274.7 2.4 fusion.12
  277.1 4.3 %convolution_convert_fusion = bf16[512,4096]{1,0:T(8,128)(2,1)} fusion(bf16[512,512]{1,0:T(8,128)(2,1)S(1)} %bitcast.177, bf16[1,512,4096]{2,1,0:T(8,128)(2,1)S(1)} %copy-done.9), kind=kOutput, calls=%fused_computation.12 | convolution fusion | flops 2149580800 | bytes 8912896 | tf_op jit(solution)/shard_map/dot_general | solution.py:172
  281.4 44.6 %reduce-scatter.2.cloned.1.call-done = bf16[512,1024]{1,0:T(8,128)(2,1)} async-done(((bf16[512,4096]{1,0:T(8,128)(2,1)}), bf16[512,1024]{1,0:T(8,128)(2,1)}) %reduce-scatter.2.cloned.1.call-update) | async-done | bytes 1048592 | tf_op jit(solution)/shard_map/reduce_scatter | solution.py:173
  326.0 5.5 %all-to-all-start.1 = ((bf16[8,64,1024]{2,1,0:T(8,128)(2,1)}), bf16[8,64,1024]{2,1,0:T(8,128)(2,1)S(1)}, u32[]{:S(2)}, u32[]{:S(2)}) async-start(bf16[8,64,1024]{2,1,0:T(8,128)(2,1)} %bitcast.164), calls=%async_computation.2 | async-start | bytes 2097152 | tf_op jit(solution)/shard_map/all_to_all | solution.py:177
  331.9 25.2 %all-to-all-done.1 = bf16[8,64,1024]{2,1,0:T(8,128)(2,1)S(1)} async-done(((bf16[8,64,1024]{2,1,0:T(8,128)(2,1)}), bf16[8,64,1024]{2,1,0:T(8,128)(2,1)S(1)}, u32[]{:S(2)}, u32[]{:S(2)}) %all-to-all-start.1) | async-done | bytes 1048608 | tf_op jit(solution)/shard_map/all_to_all | solution.py:177
  357.2 2.0 gather_fusion.1
  359.1 1.2 reshape.148
  360.4 1.4 multiply_reduce_fusion.1
  361.8 1.8 add_convert_fusion.1
  (67 shorter events, 4.1 us)
Async XLA Ops:
  6.5 153.6 %copy-start = (bf16[256,4096]{1,0:T(8,128)(2,1)S(1)}, bf16[256,4096]{1,0:T(8,128)(2,1)}, u32[]{:S(2)}) copy-start(bf16[256,4096]{1,0:T(8,128)(2,1)} %param.30) | copy-start | bytes 6291460
  6.5 6.3 %copy-start.3 = (f32[16,128]{1,0:T(8,128)S(1)}, f32[16,128]{1,0:T(8,128)}, u32[]{:S(2)}) copy-start(f32[16,128]{1,0:T(8,128)} %param.29) | copy-start | bytes 24580
  6.5 192.5 %all-reduce.30.cloned.1.call-start = ((), (), s32[]{:S(2)}) async-start(), calls=%async_computation.3 | async-start | bytes 2097152 | tf_op jit(solution)/shard_map/psum | solution.py:142
  20.9 135.3 %copy-start.6 = (f32[256]{0:T(256)S(1)}, f32[256]{0:T(256)}, u32[]{:S(2)}) copy-start(f32[256]{0:T(256)} %param.28) | copy-start | bytes 3076
  21.9 136.3 %copy-start.2 = (bf16[256,128]{1,0:T(8,128)(2,1)S(1)}, bf16[256,128]{1,0:T(8,128)(2,1)}, u32[]{:S(2)}) copy-start(bf16[256,128]{1,0:T(8,128)(2,1)} %param.20) | copy-start | bytes 196612
  156.3 5.6 %copy-start.4 = (s32[128,2]{0,1:T(2,128)S(1)}, s32[128,2]{0,1:T(2,128)}, u32[]{:S(2)}) copy-start(s32[128,2]{0,1:T(2,128)} %param.33) | copy-start | bytes 3076
  161.6 107.2 %all-gather.7.cloned.1.call-start = ((), (), s32[]{:S(2)}) async-start(), calls=%async_computation.5 | async-start | bytes 5242880 | tf_op jit(solution)/shard_map/all_gather | solution.py:167
  163.5 38.9 %dynamic-slice-start = ((f32[4096]{0:T(1024)}, s32[]{:T(128)}), f32[1024]{0:T(1024)S(1)}, s32[]{:S(2)}) async-start(f32[4096]{0:T(1024)} %param.32, s32[]{:T(128)} %select_n.74), calls=%async_computation.6 | async-start | bytes 8704 | tf_op jit(solution)/shard_map/dynamic_slice | solution.py:61
  201.0 1.3 copy-start.1
  235.4 90.6 %reduce-scatter.2.cloned.1.call-start = ((), (), s32[]{:S(2)}) async-start(), calls=%async_computation.4 | async-start | bytes 5242880 | tf_op jit(solution)/shard_map/reduce_scatter | solution.py:173
  268.8 3.4 copy-start.7
  272.3 2.3 copy-start.8
  274.6 2.5 copy-start.9
  281.4 50.4 %copy-start.5 = (f32[128,2]{0,1:T(2,128)S(1)}, f32[128,2]{0,1:T(2,128)}, u32[]{:S(2)}) copy-start(f32[128,2]{0,1:T(2,128)} %param.34) | copy-start | bytes 3076
  326.0 31.2 %all-to-all-start.1 = ((bf16[8,64,1024]{2,1,0:T(8,128)(2,1)}), bf16[8,64,1024]{2,1,0:T(8,128)(2,1)S(1)}, u32[]{:S(2)}, u32[]{:S(2)}) async-start(bf16[8,64,1024]{2,1,0:T(8,128)(2,1)} %bitcast.164), calls=%async_computation.2 | async-start | bytes 2097152 | tf_op jit(solution)/shard_map/all_to_all | solution.py:177
Sparse Core Ops, SparseCore 0:
  161.8 37.2 all-reduce.29
  235.5 33.3 all-gather.6
  281.5 44.3 reduce-scatter.1
